TPU v7x, 32 devices: a whole 2x2x4 slice. The times are simulated.
32 devices in a mesh: ep: 8 (over z, y), tp: 4 (over x, core).
Axes of the slice: x: 2, y: 2, z: 4, core: 2. Of those that a mesh axis runs over, the one named last changes fastest.
Arguments:
- value_in: bfloat16 [4096, 1024], P('ep', 'tp'), may hold values from -6 to 6
- gate_in: bfloat16 [4096, 1024], P('ep', 'tp'), may hold values from -6 to 6
- outer_gate: bfloat16 [4096, 1024], P('ep', 'tp'), may hold values from -6 to 6
- conv_weight: bfloat16 [3, 1024], P(None, 'tp'), may hold values from -3.5 to 3.5
- out_weight: bfloat16 [1024, 2048], P('tp'), may hold values from -0.1875 to 0.1875
- moe_tokens: bfloat16 [4096, 2048], P(('ep', 'tp')), may hold values from -6 to 6
- norm_gain: bfloat16 [2048], replicated, may hold values from 0.099609375 to 1.8984375
- routes: int32 [4096, 2], P(('ep', 'tp')), may hold values from 0 to 7, all different within a row; in each aligned block of 128 rows (0 to 127, 128 to 255, ...) at most 48 rows name the same one
- route_weight: float32 [4096, 2], P(('ep', 'tp')), may hold values from 0.1 to 1
- expert_gate: bfloat16 [8, 2048, 6144], P('ep', None, 'tp'), may hold values from -0.125 to 0.125
- expert_up: bfloat16 [8, 2048, 6144], P('ep', None, 'tp'), may hold values from -0.125 to 0.125
- expert_down: bfloat16 [8, 6144, 2048], P('ep', 'tp'), may hold values from -0.078125 to 0.078125
Outputs:
- mixer_out: bfloat16 [4096, 2048], P(('ep', 'tp'))
- moe_out: bfloat16 [4096, 2048], P(('ep', 'tp'))
Inputs may be any that keep to these rules, and one draw needn't show every extreme that they name: `routes`: each row names 2 different experts. Among the rows of one device no expert is named by more than 48 rows, a bound that some blocks reach.
All inputs are finite; a program needn't handle non-finite values.
Results may differ from a plain program's by a relative error of at most 0.012.
Values may be sent and summed in bfloat16 or wider, within the bound.
A program may use at most 128 MiB of HBM per device.

v0:
```python
import jax
import jax.numpy as jnp
from jax import lax
from jax.sharding import PartitionSpec as P


def extended(x, sides, width):
    for axis, dim in sides:
        size, length = (lax.axis_size(axis), x.shape[dim])
        up = [(i, (i + 1) % size) for i in range(size - 1)]
        down = [(j, i) for i, j in up]
        last = lax.slice_in_dim(x, length - width, length, axis=dim)
        leading = lax.slice_in_dim(x, 0, width, axis=dim)
        before = lax.ppermute(last, axis, up)
        after = lax.ppermute(leading, axis, down)
        x = jnp.concatenate([before, x, after], axis=dim)
    return x


def rounded(values):
    return lax.optimization_barrier(values.astype(jnp.bfloat16)).astype(jnp.float32)


def mixer_half(value_in, gate_in, outer_gate, conv_weight, out_weight):
    product = (value_in.astype(jnp.float32) * gate_in.astype(jnp.float32)).astype(jnp.bfloat16)
    padded = extended(product, (("ep", 0),), 1).astype(jnp.float32)
    taps = conv_weight.astype(jnp.float32)
    convolved = padded[:-2] * taps[0] + padded[1:-1] * taps[1] + padded[2:] * taps[2]
    mixed_rows = (outer_gate.astype(jnp.float32) * convolved).astype(jnp.bfloat16)
    return lax.psum_scatter(
        rounded(jnp.dot(mixed_rows, out_weight, preferred_element_type=jnp.float32)).astype(
            jnp.bfloat16
        ),
        "tp",
        scatter_dimension=0,
        tiled=True,
    )


def expert_half(moe_tokens, norm_gain, routes, route_weight, expert_gate, expert_up, expert_down):
    row_total, top_count = routes.shape
    features = moe_tokens.shape[1]
    local_units = expert_gate.shape[2]
    experts = lax.axis_size("ep")
    capacity = 3 * top_count * row_total // (2 * experts)
    tokens_f32 = moe_tokens.astype(jnp.float32)
    normed = (
        tokens_f32
        * lax.rsqrt(jnp.mean(tokens_f32 * tokens_f32, axis=-1, keepdims=True) + 1e-06)
        * norm_gain.astype(jnp.float32)
    ).astype(jnp.bfloat16)
    flat_ids = routes.reshape(row_total * top_count)
    matches = (flat_ids[:, None] == jnp.arange(experts, dtype=jnp.int32)[None, :]).astype(jnp.int32)
    position = jnp.sum((jnp.cumsum(matches, axis=0) - 1) * matches, axis=1)
    slot_ids = flat_ids * capacity + position
    placement = slot_ids[:, None] == jnp.arange(experts * capacity, dtype=jnp.int32)[None, :]
    placement = (
        placement.reshape(row_total, top_count, experts * capacity).sum(axis=1).astype(jnp.bfloat16)
    )
    outgoing = jnp.einsum("rs,rd->sd", placement, normed, preferred_element_type=jnp.float32)
    outgoing = outgoing.astype(jnp.bfloat16).reshape(experts, capacity, features)
    arrived = lax.all_to_all(outgoing, "ep", split_axis=0, concat_axis=0, tiled=True)
    slot_block = lax.all_gather(arrived[:, None], "tp", axis=1, tiled=True)
    lead = slot_block.shape[:-1]
    flat_rows = slot_block.reshape(-1, features)
    gate_act = jnp.dot(flat_rows, expert_gate[0], preferred_element_type=jnp.float32)
    up_act = jnp.dot(flat_rows, expert_up[0], preferred_element_type=jnp.float32)
    hidden = (jax.nn.silu(gate_act) * up_act).astype(jnp.bfloat16).reshape(lead + (local_units,))
    group_rows = experts * capacity
    group_count = group_rows * lax.axis_size("tp") // group_rows
    selected = hidden
    selected = jnp.swapaxes(selected, 0, 1).reshape(group_count * group_rows, local_units)
    summed_back = lax.psum_scatter(
        rounded(jnp.dot(selected, expert_down[0], preferred_element_type=jnp.float32)).astype(
            jnp.bfloat16
        ),
        "tp",
        scatter_dimension=0,
        tiled=True,
    )
    returned = lax.all_to_all(
        summed_back.reshape(experts, capacity, features),
        "ep",
        split_axis=0,
        concat_axis=0,
        tiled=True,
    )
    picked = returned.reshape(group_rows, features)[slot_ids].reshape(
        row_total, top_count, features
    )
    return jnp.sum(route_weight[..., None] * picked.astype(jnp.float32), axis=1).astype(
        jnp.bfloat16
    )


def body(
    value_in,
    gate_in,
    outer_gate,
    conv_weight,
    out_weight,
    moe_tokens,
    norm_gain,
    routes,
    route_weight,
    expert_gate,
    expert_up,
    expert_down,
):
    mixer_out = mixer_half(value_in, gate_in, outer_gate, conv_weight, out_weight)
    moe_out = expert_half(
        moe_tokens, norm_gain, routes, route_weight, expert_gate, expert_up, expert_down
    )
    return (mixer_out, moe_out)


def solution(mesh):
    placed = (
        P("ep", "tp"),
        P("ep", "tp"),
        P("ep", "tp"),
        P(None, "tp"),
        P("tp", None),
        P(("ep", "tp"), None),
        P(),
        P(("ep", "tp"), None),
        P(("ep", "tp"), None),
        P("ep", None, "tp"),
        P("ep", None, "tp"),
        P("ep", "tp", None),
    )
    return jax.shard_map(
        body,
        mesh=mesh,
        in_specs=placed,
        out_specs=(P(("ep", "tp"), None), P(("ep", "tp"), None)),
        check_vma=False,
    )
```

profile of v0, /device:TPU:0, one launch (start us, length us, event | category | flops | bytes accessed | tf_op | source)
XLA Modules:
  0.0 263.8 jit_solution(1294568977329746764)
XLA Ops:
  7.2 0.0 copy-start
  7.2 0.0 all-gather.3.cloned.1.call-start
  7.2 0.9 copy.22
  8.1 0.1 eq.43
  8.2 0.1 eq.39
  8.4 0.6 reduce-window.6
  9.0 0.2 slice_reduce_fusion
  9.2 0.1 fusion.20
  9.3 0.1 reduce_sum.41
  9.5 0.1 copy.25
  9.6 0.1 convert_reduce_fusion
  9.7 0.7 convert_element_type.78
  10.4 1.2 fusion.5
  11.6 1.7 convolution_convert_fusion.2
  13.3 44.2 %all_to_all.10 = bf16[8,48,2048]{2,1,0:T(8,128)(2,1)} all-to-all(bf16[8,48,2048]{2,1,0:T(8,128)(2,1)S(1)} %bitcast.33), channel_id=1, replica_groups=mesh['ep'=8,'tp'=4] {'ep'}, dimensions={0} | all-to-all | bytes 3145728 | tf_op jit(solution)/shard_map/all_to_all | solution.py:62
  57.5 0.0 slice-start
  57.5 0.0 all-gather.3.cloned.1.call-update
  57.6 0.0 reduce-scatter.5.cloned.1.call-start
  57.6 45.5 %all-gather.3.cloned.1.call-done = bf16[8,192,2048]{2,1,0:T(8,128)(2,1)} async-done(((bf16[8,48,2048]{2,1,0:T(8,128)(2,1)}), bf16[8,192,2048]{2,1,0:T(8,128)(2,1)}) %all-gather.3.cloned.1.call-update) | async-done | bytes 6291472 | tf_op jit(solution)/shard_map/all_gather | solution.py:63
  103.1 0.0 slice-start.1
  103.1 0.0 copy-start.6
  103.1 16.0 %fusion.3 = f32[1536,1536]{1,0:T(8,128)} fusion(bf16[1536,2048]{1,0:T(8,128)(2,1)} %bitcast.44, bf16[1,2048,1536]{2,1,0:T(8,128)(2,1)} %param.21), kind=kOutput, calls=%fused_computation.6 | convolution fusion | flops 9663676416 | bytes 22020096 | tf_op jit(solution)/shard_map/dot_general | solution.py:66
  119.1 0.0 slice-done
  119.1 0.0 slice-done.1
  119.1 0.0 copy-done.6
  119.1 13.8 %fusion = bf16[1536,1536]{1,0:T(8,128)(2,1)S(1)} fusion(bf16[1536,2048]{1,0:T(8,128)(2,1)S(1)} %bitcast.45, f32[1536,1536]{1,0:T(8,128)} %fusion.3, bf16[1,2048,1536]{2,1,0:T(8,128)(2,1)S(1)} %bitcast.43), kind=kOutput, calls=%fused_computation.2 | convolution fusion | flops 9677832192 | bytes 26738688 | tf_op jit(solution)/shard_map/dot_general | solution.py:67
  132.9 0.4 copy.26
  133.3 13.8 %convolution_convert_fusion = bf16[1536,2048]{1,0:T(8,128)(2,1)} fusion(bf16[1536,1536]{1,0:T(8,128)(2,1)S(1)} %bitcast.35, bf16[1,1536,2048]{2,1,0:T(8,128)(2,1)} %param.23), kind=kOutput, calls=%fused_computation.3 | convolution fusion | flops 9666822144 | bytes 17301504 | tf_op jit(solution)/shard_map/dot_general | solution.py:74
  147.1 0.0 copy-start.1
  147.1 0.0 copy-start.2
  147.1 0.0 copy-start.4
  147.1 0.0 copy-start.3
  147.1 0.0 reduce-scatter.5.cloned.1.call-update
  147.2 0.0 copy-start.5
  147.2 0.0 reduce-scatter.3.cloned.1.call-start
  147.2 0.9 copy-done.1
  148.1 0.1 copy-done.2
  148.2 0.1 multiply_convert_fusion
  148.2 3.4 %collective-permute-start = (bf16[1,256]{1,0:T(2,128)(2,1)S(1)}, bf16[1,256]{1,0:T(2,128)(2,1)S(1)}, u32[]{:S(2)}, u32[]{:S(2)}) collective-permute-start(bf16[1,256]{1,0:T(2,128)(2,1)S(1)} %get-tuple-element.2), channel_id=1, source_target_pairs={{0,4},{4,8},{8,12},{12,16},{16,20},{20,24},{24,28},{1,5},{5,9},{9,... | collective-permute-start | bytes 1544 | tf_op jit(solution)/shard_map/ppermute | solution.py:14
  151.6 1.3 collective-permute-start.1
  152.9 0.0 copy-done.4
  152.9 0.0 collective-permute-done
  153.0 4.1 %collective-permute-done.1 = bf16[1,256]{1,0:T(2,128)(2,1)S(1)} collective-permute-done((bf16[1,256]{1,0:T(2,128)(2,1)S(1)}, bf16[1,256]{1,0:T(2,128)(2,1)S(1)}, u32[]{:S(2)}, u32[]{:S(2)}) %collective-permute-start.1) | collective-permute-done | bytes 544 | tf_op jit(solution)/shard_map/ppermute | solution.py:15
  157.1 0.1 maximum_convert_fusion
  157.1 0.0 copy-done
  157.2 0.0 copy-done.3
  157.2 2.2 convolution_convert_fusion.1
  159.3 0.0 reduce-scatter.3.cloned.1.call-update
  159.3 46.8 %reduce-scatter.5.cloned.1.call-done = bf16[384,2048]{1,0:T(8,128)(2,1)} async-done(((bf16[1536,2048]{1,0:T(8,128)(2,1)}), bf16[384,2048]{1,0:T(8,128)(2,1)}) %reduce-scatter.5.cloned.1.call-update) | async-done | bytes 1572880 | tf_op jit(solution)/shard_map/reduce_scatter | solution.py:73
  206.2 5.5 %all-to-all-start.1 = ((bf16[8,48,2048]{2,1,0:T(8,128)(2,1)}), bf16[8,48,2048]{2,1,0:T(8,128)(2,1)S(1)}, u32[]{:S(2)}, u32[]{:S(2)}) async-start(bf16[8,48,2048]{2,1,0:T(8,128)(2,1)} %bitcast.36), calls=%async_computation.3 | async-start | bytes 3145728 | tf_op jit(solution)/shard_map/all_to_all | solution.py:81
  211.7 0.1 mul.114
  211.8 0.0 copy-done.5
  211.8 0.1 copy.21
  212.0 36.6 %all-to-all-done.1 = bf16[8,48,2048]{2,1,0:T(8,128)(2,1)S(1)} async-done(((bf16[8,48,2048]{2,1,0:T(8,128)(2,1)}), bf16[8,48,2048]{2,1,0:T(8,128)(2,1)S(1)}, u32[]{:S(2)}, u32[]{:S(2)}) %all-to-all-start.1) | async-done | bytes 1572896 | tf_op jit(solution)/shard_map/all_to_all | solution.py:81
  248.5 2.3 gather_fusion
  250.9 2.4 reshape.104
  253.3 4.0 %multiply_reduce_fusion = bf16[128,2048]{1,0:T(8,128)(2,1)} fusion(f32[128,2,2048]{2,1,0:T(2,128)S(1)} %reshape.104, f32[128,2]{1,0:T(8,128)S(1)} %copy.21), kind=kLoop, calls=%fused_computation.10 | loop fusion | flops 786432 | bytes 2622464 | tf_op jit(solution)/shard_map/reduce_sum | solution.py:91
  257.3 0.0 reduce-scatter.3.cloned.1.call-done
  (10 shorter events, 0.1 us)
Async XLA Ops:
  7.2 150.0 %copy-start = (bf16[256,2048]{1,0:T(8,128)(2,1)S(1)}, bf16[256,2048]{1,0:T(8,128)(2,1)}, u32[]{:S(2)}) copy-start(bf16[256,2048]{1,0:T(8,128)(2,1)} %param.16) | copy-start | bytes 3145732
  7.2 95.9 %all-gather.3.cloned.1.call-start = ((), (), s32[]{:S(2)}) async-start(), calls=%async_computation.6 | async-start | bytes 7864320 | tf_op jit(solution)/shard_map/all_gather | solution.py:63
  57.5 61.6 %slice-start = ((s8[6291456]{0:T(1024)(128)(4,1)}), s8[2097152]{0:T(1024)(128)(4,1)S(1)}, s32[]{:S(2)}) async-start(s8[6291456]{0:T(1024)(128)(4,1)} %bitcast.42), calls=%async_computation.7 | async-start | bytes 4194304
  57.6 148.6 %reduce-scatter.5.cloned.1.call-start = ((), (), s32[]{:S(2)}) async-start(), calls=%async_computation.5 | async-start | bytes 7864320 | tf_op jit(solution)/shard_map/reduce_scatter | solution.py:73
  103.1 16.1 %slice-start.1 = ((s8[6291456]{0:T(1024)(128)(4,1)}), s8[4194304]{0:T(1024)(128)(4,1)S(1)}, s32[]{:S(2)}) async-start(s8[6291456]{0:T(1024)(128)(4,1)} %bitcast.42), calls=%async_computation.8 | async-start | bytes 8388608
  103.1 16.1 %copy-start.6 = (bf16[8,192,2048]{2,1,0:T(8,128)(2,1)S(1)}, bf16[8,192,2048]{2,1,0:T(8,128)(2,1)}, u32[]{:S(2)}) copy-start(bf16[8,192,2048]{2,1,0:T(8,128)(2,1)} %all-gather.3.cloned.1.call-done) | copy-start | bytes 18874372
  147.1 0.9 copy-start.1
  147.1 1.0 copy-start.2
  147.1 5.8 %copy-start.4 = (bf16[3,256]{1,0:T(4,128)(2,1)S(1)}, bf16[3,256]{1,0:T(4,128)(2,1)}, u32[]{:S(2)}) copy-start(bf16[3,256]{1,0:T(4,128)(2,1)} %param.15) | copy-start | bytes 4612
  147.1 10.0 %copy-start.3 = (bf16[512,256]{1,0:T(8,128)(2,1)S(1)}, bf16[512,256]{1,0:T(8,128)(2,1)}, u32[]{:S(2)}) copy-start(bf16[512,256]{1,0:T(8,128)(2,1)} %param.14) | copy-start | bytes 786436
  147.2 64.7 %copy-start.5 = (f32[128,2]{0,1:T(2,128)S(1)}, f32[128,2]{0,1:T(2,128)}, u32[]{:S(2)}) copy-start(f32[128,2]{0,1:T(2,128)} %param.20) | copy-start | bytes 3076
  147.2 110.1 %reduce-scatter.3.cloned.1.call-start = ((), (), s32[]{:S(2)}) async-start(), calls=%async_computation.4 | async-start | bytes 2621440 | tf_op jit(solution)/shard_map/reduce_scatter | solution.py:30
  148.2 4.7 %collective-permute-start = (bf16[1,256]{1,0:T(2,128)(2,1)S(1)}, bf16[1,256]{1,0:T(2,128)(2,1)S(1)}, u32[]{:S(2)}, u32[]{:S(2)}) collective-permute-start(bf16[1,256]{1,0:T(2,128)(2,1)S(1)} %get-tuple-element.2), channel_id=1, source_target_pairs={{0,4},{4,8},{8,12},{12,16},{16,20},{20,24},{24,28},{1,5},{5,9},{9,... | collective-permute-start | bytes 1544 | tf_op jit(solution)/shard_map/ppermute | solution.py:14
  151.6 5.5 %collective-permute-start.1 = (bf16[1,256]{1,0:T(2,128)(2,1)S(1)}, bf16[1,256]{1,0:T(2,128)(2,1)S(1)}, u32[]{:S(2)}, u32[]{:S(2)}) collective-permute-start(bf16[1,256]{1,0:T(2,128)(2,1)S(1)} %get-tuple-element.3), channel_id=1, source_target_pairs={{4,0},{8,4},{12,8},{16,12},{20,16},{24,20},{28,24},{5,1},{9,5},{13... | collective-permute-start | bytes 1544 | tf_op jit(solution)/shard_map/ppermute | solution.py:15
  206.2 42.4 %all-to-all-start.1 = ((bf16[8,48,2048]{2,1,0:T(8,128)(2,1)}), bf16[8,48,2048]{2,1,0:T(8,128)(2,1)S(1)}, u32[]{:S(2)}, u32[]{:S(2)}) async-start(bf16[8,48,2048]{2,1,0:T(8,128)(2,1)} %bitcast.36), calls=%async_computation.3 | async-start | bytes 3145728 | tf_op jit(solution)/shard_map/all_to_all | solution.py:81
Sparse Core Ops, SparseCore 0:
  57.7 45.3 all-gather.2
  147.3 58.8 reduce-scatter.4
  209.3 31.1 reduce-scatter.2
where the time goes:
time: 264 us
  waiting for transfers between devices  133 us (50%)
  matrix products  47.5 us (18%)
  blocking collectives  44.2 us (17%)
  between operations  13.9 us (5%)
  starting transfers between devices  10.3 us (4%)
  local copies, waits for them, and re-layouts  7.91 us (3%)
  other arithmetic  6.96 us (3%)
    reduce_scatter x1, waiting for transfers between devices, expert_half(): lax.psum_scatter(rounded(jnp.dot(selected, expert_down[0], preferred_elem...  46.8 us
    all_gather x1, waiting for transfers between devices, expert_half(): slot_block = lax.all_gather(arrived[:, None], 'tp', axis=1, tiled=True)  45.5 us
    all_to_all x1, blocking collectives, expert_half(): lax.all_to_all(outgoing, 'ep', split_axis=0, concat_axis=0, tiled=True)  44.2 us
    all_to_all x1, waiting for transfers between devices, expert_half(): lax.all_to_all(summed_back.reshape(experts, capacity, features), 'ep', sp...  36.6 us
    dot_general x1, matrix products, expert_half(): jnp.dot(flat_rows, expert_gate[0], preferred_element_type=jnp.float32)  16 us
    dot_general x1, matrix products, expert_half(): jnp.dot(selected, expert_down[0], preferred_element_type=jnp.float32)  13.8 us
    dot_general x1, matrix products, expert_half(): jnp.dot(flat_rows, expert_up[0], preferred_element_type=jnp.float32)  13.8 us
    all_to_all x1, starting transfers between devices, expert_half(): lax.all_to_all(summed_back.reshape(experts, capacity, features), 'ep', sp...  5.52 us
  transfers between devices with their start and end apart: 6, of which 4 were waited for; matrix products, arithmetic and copies ran while one was open for 4% of the time, Pallas kernels for 0%

commit v1 on v0

v1 whole, which is shorter than its diff:
```python
import functools

import jax
import jax.numpy as jnp
from jax import lax
from jax.experimental import pallas as pl
from jax.experimental.pallas import tpu as pltpu
from jax.sharding import PartitionSpec as P


def extended(x, sides, width):
    for axis, dim in sides:
        size, length = (lax.axis_size(axis), x.shape[dim])
        up = [(i, (i + 1) % size) for i in range(size - 1)]
        down = [(j, i) for i, j in up]
        last = lax.slice_in_dim(x, length - width, length, axis=dim)
        leading = lax.slice_in_dim(x, 0, width, axis=dim)
        before = lax.ppermute(last, axis, up)
        after = lax.ppermute(leading, axis, down)
        x = jnp.concatenate([before, x, after], axis=dim)
    return x


def rounded(values):
    return lax.optimization_barrier(values.astype(jnp.bfloat16)).astype(jnp.float32)


def mixer_half(value_in, gate_in, outer_gate, conv_weight, out_weight):
    product = (value_in.astype(jnp.float32) * gate_in.astype(jnp.float32)).astype(jnp.bfloat16)
    padded = extended(product, (("ep", 0),), 1).astype(jnp.float32)
    taps = conv_weight.astype(jnp.float32)
    convolved = padded[:-2] * taps[0] + padded[1:-1] * taps[1] + padded[2:] * taps[2]
    mixed_rows = (outer_gate.astype(jnp.float32) * convolved).astype(jnp.bfloat16)
    return rounded(jnp.dot(mixed_rows, out_weight, preferred_element_type=jnp.float32)).astype(
        jnp.bfloat16
    )


MESH = pl.DeviceIdType.MESH


def expert_kernel(
    experts, shards, cap, tile,
    sent, gate_hbm, up_hbm, down_hbm, back,
    gate_w, up_w, down_w, slots, hidden, part, core_in, pair, chip_in, total,
    w_sem, own_sem, out_s, out_r, xf_s, xf_r, df_s, df_r, dr_s, dr_r, xr_s, xr_r, bk_s, bk_r,
):
    stages = experts // 2
    high = shards // 2
    me, mine = lax.axis_index("ep"), lax.axis_index("tp")
    low, top = lax.rem(mine, 2), mine // 2
    partner = (me, mine + 1 - 2 * low)
    across = (me, lax.rem(mine + high, shards))
    wide, half = 2 * cap, 2 * high * cap
    own_half = pl.multiple_of(low * half, 16)
    other_half = pl.multiple_of((1 - low) * half, 16)
    own_top = pl.multiple_of(top * wide, 16)
    other_top = pl.multiple_of((1 - top) * wide, 16)

    def to(k):
        return lax.rem(me + k, experts)

    def source(k):
        return lax.rem(me + experts - k, experts)

    def place(k):
        return pl.ds(pl.multiple_of(own_half + own_top + (k % 2) * cap, 16), cap)

    def remote(src, dst, s, r, device):
        return pltpu.make_async_remote_copy(
            src_ref=src, dst_ref=dst, send_sem=s, recv_sem=r, device_id=device, device_id_type=MESH
        )

    loads = [
        pltpu.make_async_copy(a, b, w_sem.at[i])
        for i, (a, b) in enumerate(((gate_hbm, gate_w), (up_hbm, up_w), (down_hbm, down_w)))
    ]
    barrier = pltpu.get_barrier_semaphore()
    for k in range(1, experts):
        pl.semaphore_signal(barrier, inc=1, device_id=(to(k), mine), device_id_type=MESH)
    for device in (partner, across):
        pl.semaphore_signal(barrier, inc=1, device_id=device, device_id_type=MESH)
    for load in loads:
        load.start()
    own_in = pltpu.make_async_copy(sent.at[me], slots.at[0, place(0)], own_sem.at[0])
    own_in.start()
    pl.semaphore_wait(barrier, experts + 1)

    out = [None] + [
        remote(sent.at[to(k)], slots.at[k // 2, place(k)], out_s.at[k], out_r.at[k], (to(k), mine))
        for k in range(1, experts)
    ]
    for copy in out[1:]:
        copy.start()
    x_out = [
        remote(slots.at[k // 2, place(k)], slots.at[k // 2, place(k)], xf_s.at[k], xf_r.at[k], across)
        for k in range(experts)
    ]
    rows = pl.ds(own_half, half)
    d_out = [
        remote(slots.at[j, rows], slots.at[j, rows], df_s.at[j], df_r.at[j], partner)
        for j in range(stages)
    ]
    d_back = [
        remote(part.at[j, pl.ds(other_half, half)], core_in.at[j], dr_s.at[j], dr_r.at[j], partner)
        for j in range(stages)
    ]
    x_back = [
        remote(pair.at[j, pl.ds(other_top, wide)], chip_in.at[j], xr_s.at[j], xr_r.at[j], across)
        for j in range(stages)
    ]
    own_out = pltpu.make_async_copy(total.at[0, pl.ds(0, cap)], back.at[me], own_sem.at[1])
    home = [own_out] + [
        remote(
            total.at[k // 2, pl.ds((k % 2) * cap, cap)], back.at[me], bk_s.at[k], bk_r.at[k],
            (source(k), mine),
        )
        for k in range(1, experts)
    ]

    def arrive(j):
        for k in (2 * j, 2 * j + 1):
            if k == 0:
                own_in.wait()
            else:
                out[k].wait_recv()
            x_out[k].start()

    def spread(j):
        x_out[2 * j].wait_recv()
        x_out[2 * j + 1].wait_recv()
        d_out[j].start()

    def activate(j):
        d_out[j].wait_recv()

        def step(i, carry):
            at = pl.ds(pl.multiple_of(i * tile, tile), tile)
            x = slots[j]
            g = jnp.dot(x, gate_w[:, at], preferred_element_type=jnp.float32)
            u = jnp.dot(x, up_w[:, at], preferred_element_type=jnp.float32)
            hidden[:, at] = (g / (1.0 + jnp.exp(-g)) * u).astype(jnp.bfloat16)
            return carry

        lax.fori_loop(0, gate_w.shape[1] // tile, step, 0)

    def project(j):
        def step(i, carry):
            at = pl.ds(pl.multiple_of(i * tile, tile), tile)
            part[j, :, at] = jnp.dot(
                hidden[...], down_w[:, at], preferred_element_type=jnp.float32
            ).astype(jnp.bfloat16)
            return carry

        lax.fori_loop(0, down_w.shape[1] // tile, step, 0)
        d_back[j].start()

    def pair_up(j):
        d_back[j].wait_recv()
        pair[j] = (
            part[j, pl.ds(own_half, half)].astype(jnp.float32) + core_in[j].astype(jnp.float32)
        ).astype(jnp.bfloat16)
        x_back[j].start()

    def finish(j):
        x_back[j].wait_recv()
        total[j] = (
            pair[j, pl.ds(own_top, wide)].astype(jnp.float32) + chip_in[j].astype(jnp.float32)
        ).astype(jnp.bfloat16)
        home[2 * j].start()
        home[2 * j + 1].start()

    arrive(0)
    spread(0)
    for j in range(stages):
        if j + 1 < stages:
            arrive(j + 1)
        if j == 0:
            loads[0].wait()
            loads[1].wait()
        activate(j)
        if j + 1 < stages:
            spread(j + 1)
        if j >= 1:
            pair_up(j - 1)
        if j >= 2:
            finish(j - 2)
        if j == 0:
            loads[2].wait()
        project(j)
    pair_up(stages - 1)
    if stages >= 2:
        finish(stages - 2)
    finish(stages - 1)
    own_out.wait()
    for k in range(1, experts):
        out[k].wait_send()
        home[k].wait()
    for k in range(experts):
        x_out[k].wait_send()
    for j in range(stages):
        d_out[j].wait_send()
        d_back[j].wait_send()
        x_back[j].wait_send()


def expert_half(
    partial_rows, moe_tokens, norm_gain, routes, route_weight, expert_gate, expert_up, expert_down
):
    row_total, top_count = routes.shape
    features = moe_tokens.shape[1]
    local_units = expert_gate.shape[2]
    experts, shards = lax.axis_size("ep"), lax.axis_size("tp")
    capacity = 3 * top_count * row_total // (2 * experts)
    capacity = -(-capacity // 16) * 16
    slots = experts * capacity
    tokens_f32 = moe_tokens.astype(jnp.float32)
    normed = (
        tokens_f32
        * lax.rsqrt(jnp.mean(tokens_f32 * tokens_f32, axis=-1, keepdims=True) + 1e-06)
        * norm_gain.astype(jnp.float32)
    ).astype(jnp.bfloat16)
    chosen = routes[:, :, None] == jnp.arange(experts, dtype=jnp.int32)[None, None, :]
    named = chosen.any(axis=1).astype(jnp.bfloat16)
    before = jnp.arange(row_total)[:, None] > jnp.arange(row_total)[None, :]
    rank = jnp.dot(before.astype(jnp.bfloat16), named, preferred_element_type=jnp.float32)
    position = jnp.sum(jnp.where(chosen, rank[:, None, :], 0.0), axis=2).astype(jnp.int32)
    slot_ids = routes * capacity + position
    at_slot = slot_ids[:, :, None] == jnp.arange(slots, dtype=jnp.int32)[None, None, :]
    placement = at_slot.any(axis=1).astype(jnp.bfloat16)
    outgoing = jnp.einsum("rs,rd->sd", placement, normed, preferred_element_type=jnp.float32)
    outgoing = outgoing.astype(jnp.bfloat16).reshape(experts, capacity, features)
    outgoing, partial_rows = lax.optimization_barrier((outgoing, partial_rows))
    mixer_out = lax.psum_scatter(partial_rows, "tp", scatter_dimension=0, tiled=True)
    stages, rows = experts // 2, 2 * shards * capacity
    bf16 = jnp.bfloat16
    dma = pltpu.SemaphoreType.DMA
    returned = pl.pallas_call(
        functools.partial(expert_kernel, experts, shards, capacity, 256),
        out_shape=jax.ShapeDtypeStruct((experts, capacity, features), bf16),
        in_specs=[pl.BlockSpec(memory_space=pltpu.VMEM)] + [pl.BlockSpec(memory_space=pl.ANY)] * 3,
        out_specs=pl.BlockSpec(memory_space=pltpu.VMEM),
        scratch_shapes=[
            pltpu.VMEM((features, local_units), bf16),
            pltpu.VMEM((features, local_units), bf16),
            pltpu.VMEM((local_units, features), bf16),
            pltpu.VMEM((stages, rows, features), bf16),
            pltpu.VMEM((rows, local_units), bf16),
            pltpu.VMEM((stages, rows, features), bf16),
            pltpu.VMEM((stages, rows // 2, features), bf16),
            pltpu.VMEM((stages, rows // 2, features), bf16),
            pltpu.VMEM((stages, rows // shards, features), bf16),
            pltpu.VMEM((stages, rows // shards, features), bf16),
            dma((3,)),
            dma((2,)),
        ]
        + [dma((experts,))] * 4
        + [dma((stages,))] * 6
        + [dma((experts,))] * 2,
        compiler_params=pltpu.CompilerParams(
            collective_id=0, has_side_effects=True, vmem_limit_bytes=60 * 2**20
        ),
        cost_estimate=pl.CostEstimate(
            flops=6 * stages * rows * features * local_units,
            bytes_accessed=6 * features * local_units,
            transcendentals=stages * rows * local_units,
        ),
    )(outgoing, expert_gate[0], expert_up[0], expert_down[0])
    weights = jnp.sum(jnp.where(at_slot, route_weight[:, :, None], 0.0), axis=1)
    leading = weights.astype(bf16)
    trailing = (weights - leading.astype(jnp.float32)).astype(bf16)
    result = returned.reshape(slots, features)
    moe_out = jnp.dot(leading, result, preferred_element_type=jnp.float32) + jnp.dot(
        trailing, result, preferred_element_type=jnp.float32
    )
    return mixer_out, moe_out.astype(bf16)


def body(
    value_in,
    gate_in,
    outer_gate,
    conv_weight,
    out_weight,
    moe_tokens,
    norm_gain,
    routes,
    route_weight,
    expert_gate,
    expert_up,
    expert_down,
):
    partial_rows = mixer_half(value_in, gate_in, outer_gate, conv_weight, out_weight)
    return expert_half(
        partial_rows,
        moe_tokens,
        norm_gain,
        routes,
        route_weight,
        expert_gate,
        expert_up,
        expert_down,
    )


def solution(mesh):
    placed = (
        P("ep", "tp"),
        P("ep", "tp"),
        P("ep", "tp"),
        P(None, "tp"),
        P("tp", None),
        P(("ep", "tp"), None),
        P(),
        P(("ep", "tp"), None),
        P(("ep", "tp"), None),
        P("ep", None, "tp"),
        P("ep", None, "tp"),
        P("ep", "tp", None),
    )
    return jax.shard_map(
        body,
        mesh=mesh,
        in_specs=placed,
        out_specs=(P(("ep", "tp"), None), P(("ep", "tp"), None)),
        check_vma=False,
    )
```

time: 264 us -> 151 us (0.57)
  waiting for transfers between devices: 133 us -> 0.02 us
  Pallas kernels: 0 us -> 116 us
  blocking collectives: 44.2 us -> 0 us
  matrix products: 47.5 us -> 7.31 us
  local copies, waits for them, and re-layouts: 7.91 us -> 0.7 us
  starting transfers between devices: 10.3 us -> 6.86 us
    pallas_call x0 -> x1, Pallas kernels: none -> 116 us  [expert_half(): pl.pallas_call(functools.partial(expert_kernel, experts, shards, capacity...]
    reduce_scatter x2 -> x1, waiting for transfers between devices: 46.8 us -> 0.01 us  [expert_half(): lax.psum_scatter(partial_rows, 'tp', scatter_dimension=0, tiled=True)]
    all_gather x1 -> x0, waiting for transfers between devices: 45.5 us -> none  [expert_half(): slot_block = lax.all_gather(arrived[:, None], 'tp', axis=1, tiled=True)]
    all_to_all x1 -> x0, blocking collectives: 44.2 us -> none  [expert_half(): lax.all_to_all(outgoing, 'ep', split_axis=0, concat_axis=0, tiled=True)]
    dot_general x3, matrix products: 43.6 us -> 3.33 us  [the longest x1 1.96 us: expert_half(): jnp.dot(leading, result, preferred_element_type=jnp.float32)]
    all_to_all x1 -> x0, waiting for transfers between devices: 36.6 us -> none  [expert_half(): lax.all_to_all(summed_back.reshape(experts, capacity, features), 'ep', sp...]
    all_to_all x1 -> x0, starting transfers between devices: 5.52 us -> none  [expert_half(): lax.all_to_all(summed_back.reshape(experts, capacity, features), 'ep', sp...]
    ppermute x1, waiting for transfers between devices: 4.13 us -> 0.01 us  [extended(): after = lax.ppermute(leading, axis, down)]
  transfers between devices with their start and end apart: 6 -> 3, of which waited for: 4 -> 0; matrix products, arithmetic and copies ran while one was open for 4% -> 6% of each run, Pallas kernels for 0% -> 77%
where the time goes in v1:
time: 151 us
  Pallas kernels  116 us (77%)
  between operations  14.2 us (9%)
  matrix products  7.31 us (5%)
  starting transfers between devices  6.86 us (5%)
  other arithmetic  5.52 us (4%)
    pallas_call x1, Pallas kernels, expert_half(): pl.pallas_call(functools.partial(expert_kernel, experts, shards, capacity...  116 us
    ppermute x1, starting transfers between devices, extended(): before = lax.ppermute(last, axis, up)  5.53 us
  transfers between devices with their start and end apart: 3, of which 0 were waited for; matrix products, arithmetic and copies ran while one was open for 6% of the time, Pallas kernels for 77%

profile of v1, /device:TPU:0, one launch (start us, length us, event | category | flops | bytes accessed | tf_op | source)
XLA Modules:
  0.0 150.7 jit_solution(14316449143697903437)
XLA Ops:
  7.2 0.0 copy-start
  7.2 0.0 copy-start.2
  7.2 0.0 reduce-scatter.2.cloned.1.call-start
  7.2 1.2 multiply_convert_fusion
  8.5 0.0 copy-start.4
  8.5 1.3 collective-permute-start.1
  9.8 5.5 %collective-permute-start = (bf16[1,256]{1,0:T(2,128)(2,1)S(1)}, bf16[1,256]{1,0:T(2,128)(2,1)S(1)}, u32[]{:S(2)}, u32[]{:S(2)}) collective-permute-start(bf16[1,256]{1,0:T(2,128)(2,1)S(1)} %get-tuple-element.6), channel_id=1, source_target_pairs={{0,4},{4,8},{8,12},{12,16},{16,20},{20,24},{24,28},{1,5},{5,9},{9,... | collective-permute-start | bytes 1544 | tf_op jit(solution)/shard_map/ppermute | solution.py:18
  15.3 0.7 fusion.20
  16.0 0.1 fusion.16
  16.1 0.7 select_reduce_fusion.1
  16.9 0.7 convert_add_fusion
  17.5 0.1 fusion.11
  17.6 0.7 convert_element_type.58
  18.3 1.2 fusion.1
  19.6 0.0 copy-start.3
  19.6 0.0 copy-done.2
  19.6 1.8 %convolution_convert_fusion.1 = bf16[384,2048]{1,0:T(8,128)(2,1)} fusion(pred[128,384]{1,0:T(8,128)(4,1)S(1)} %fusion.11, bf16[128,2048]{1,0:T(8,128)(2,1)S(1)} %copy-done.2, f32[2048]{0:T(1024)S(1)} %convert_element_type.58, f32[128]{0:T(128)S(1)} %add_rsqrt_fusion), kind=kOutput, calls=%fused_computation.1 | convolution fusion | flops 203161600 | bytes 2155008 | tf_op jit(solution)/shard_map/rs,rd->sd/dot_general | solution.py:231
  21.4 0.0 copy-done.4
  21.4 0.0 collective-permute-done.1
  21.4 0.0 collective-permute-done
  21.4 0.1 maximum_convert_fusion
  21.5 0.0 copy-done
  21.5 0.0 copy-done.3
  21.5 2.2 %convolution_convert_fusion = bf16[512,2048]{1,0:T(8,128)(2,1)} fusion(bf16[256,2048]{1,0:T(8,128)(2,1)S(1)} %copy-done, f32[514,256]{1,0:T(8,128)S(1)} %maximum_convert_fusion, bf16[512,256]{1,0:T(8,128)(2,1)S(1)} %copy-done.3, f32[256]{0:T(256)S(1)} %bitcast.18, f32[256]{0:T(256)S(1)} %bitcast.17, f32[256]{0:T(256)S(1)} %bitcast.16), kind=kOutput, calls=%fused_computation | convolution fusion | flops 538968064 | bytes 4983808 | tf_op jit(solution)/shard_map/dot_general | solution.py:34
  23.7 0.0 copy-start.5
  23.7 0.0 reduce-scatter.2.cloned.1.call-update
  23.7 0.7 copy-done.5
  24.4 0.1 select_reduce_fusion
  24.5 116.1 %shard_map.131 = bf16[8,48,2048]{2,1,0:T(8,128)(2,1)} custom-call(bf16[8,48,2048]{2,1,0:T(8,128)(2,1)} %bitcast.15, bf16[2048,1536]{1,0:T(8,128)(2,1)} %bitcast.19, bf16[2048,1536]{1,0:T(8,128)(2,1)} %bitcast.20, bf16[1536,2048]{1,0:T(8,128)(2,1)} %bitcast.21), custom_call_target="tpu_custom_call" | custom-call | flops 28991029248 | bytes 18874368 | tf_op jit(solution)/shard_map/pallas_call | solution.py:238
  140.6 0.0 copy-start.1
  140.7 2.0 %fusion.18 = f32[128,2048]{1,0:T(8,128)S(1)} fusion(bf16[384,2048]{1,0:T(8,128)(2,1)} %bitcast.13, f32[128,384]{1,0:T(8,128)S(1)} %select_reduce_fusion), kind=kOutput, calls=%fused_computation.30 | convolution fusion | flops 201375744 | bytes 2818048 | tf_op jit(solution)/shard_map/dot_general | solution.py:273
  142.6 0.0 copy-done.1
  142.6 1.2 fusion
  143.9 0.0 reduce-scatter.2.cloned.1.call-done
  (3 shorter events, 0.0 us)
Async XLA Ops:
  7.2 14.3 %copy-start = (bf16[256,2048]{1,0:T(8,128)(2,1)S(1)}, bf16[256,2048]{1,0:T(8,128)(2,1)}, u32[]{:S(2)}) copy-start(bf16[256,2048]{1,0:T(8,128)(2,1)} %param.16) | copy-start | bytes 3145732
  7.2 12.4 %copy-start.2 = (bf16[128,2048]{1,0:T(8,128)(2,1)S(1)}, bf16[128,2048]{1,0:T(8,128)(2,1)}, u32[]{:S(2)}) copy-start(bf16[128,2048]{1,0:T(8,128)(2,1)} %param.17) | copy-start | bytes 1572868
  7.2 136.7 %reduce-scatter.2.cloned.1.call-start = ((), (), s32[]{:S(2)}) async-start(), calls=%async_computation.1 | async-start | bytes 2621440 | tf_op jit(solution)/shard_map/reduce_scatter | solution.py:234
  8.5 13.0 %copy-start.4 = (bf16[3,256]{1,0:T(4,128)(2,1)S(1)}, bf16[3,256]{1,0:T(4,128)(2,1)}, u32[]{:S(2)}) copy-start(bf16[3,256]{1,0:T(4,128)(2,1)} %param.15) | copy-start | bytes 4612
  8.5 12.9 %collective-permute-start.1 = (bf16[1,256]{1,0:T(2,128)(2,1)S(1)}, bf16[1,256]{1,0:T(2,128)(2,1)S(1)}, u32[]{:S(2)}, u32[]{:S(2)}) collective-permute-start(bf16[1,256]{1,0:T(2,128)(2,1)S(1)} %get-tuple-element.7), channel_id=1, source_target_pairs={{4,0},{8,4},{12,8},{16,12},{20,16},{24,20},{28,24},{5,1},{9,5},{13... | collective-permute-start | bytes 1544 | tf_op jit(solution)/shard_map/ppermute | solution.py:19
  9.8 11.6 %collective-permute-start = (bf16[1,256]{1,0:T(2,128)(2,1)S(1)}, bf16[1,256]{1,0:T(2,128)(2,1)S(1)}, u32[]{:S(2)}, u32[]{:S(2)}) collective-permute-start(bf16[1,256]{1,0:T(2,128)(2,1)S(1)} %get-tuple-element.6), channel_id=1, source_target_pairs={{0,4},{4,8},{8,12},{12,16},{16,20},{20,24},{24,28},{1,5},{5,9},{9,... | collective-permute-start | bytes 1544 | tf_op jit(solution)/shard_map/ppermute | solution.py:18
  19.6 1.9 %copy-start.3 = (bf16[512,256]{1,0:T(8,128)(2,1)S(1)}, bf16[512,256]{1,0:T(8,128)(2,1)}, u32[]{:S(2)}) copy-start(bf16[512,256]{1,0:T(8,128)(2,1)} %param.14) | copy-start | bytes 786436
  23.7 0.7 copy-start.5
  140.6 2.0 %copy-start.1 = (bf16[8,48,2048]{2,1,0:T(8,128)(2,1)S(1)}, bf16[8,48,2048]{2,1,0:T(8,128)(2,1)}, u32[]{:S(2)}) copy-start(bf16[8,48,2048]{2,1,0:T(8,128)(2,1)} %shard_map.131) | copy-start | bytes 4718596
Sparse Core Ops, SparseCore 0:
  23.8 38.1 reduce-scatter.1

commit v2 on v1

--- a/solution.py
+++ b/solution.py
@@ -106,8 +106,11 @@
         for j in range(stages)
     ]
     x_back = [
-        remote(pair.at[j, pl.ds(other_top, wide)], chip_in.at[j], xr_s.at[j], xr_r.at[j], across)
-        for j in range(stages)
+        remote(
+            pair.at[k // 2, pl.ds(pl.multiple_of(other_top + (k % 2) * cap, 16), cap)],
+            chip_in.at[k // 2, pl.ds((k % 2) * cap, cap)], xr_s.at[k], xr_r.at[k], across,
+        )
+        for k in range(experts)
     ]
     own_out = pltpu.make_async_copy(total.at[0, pl.ds(0, cap)], back.at[me], own_sem.at[1])
     home = [own_out] + [
@@ -155,20 +158,29 @@
         lax.fori_loop(0, down_w.shape[1] // tile, step, 0)
         d_back[j].start()
 
+    def add_pair(j, first, count):
+        mine_rows = pl.ds(pl.multiple_of(own_half + first, 16), count)
+        pair[j, pl.ds(first, count)] = (
+            part[j, mine_rows].astype(jnp.float32)
+            + core_in[j, pl.ds(first, count)].astype(jnp.float32)
+        ).astype(jnp.bfloat16)
+
     def pair_up(j):
         d_back[j].wait_recv()
-        pair[j] = (
-            part[j, pl.ds(own_half, half)].astype(jnp.float32) + core_in[j].astype(jnp.float32)
-        ).astype(jnp.bfloat16)
-        x_back[j].start()
+        for k in (2 * j, 2 * j + 1):
+            add_pair(j, pl.multiple_of(other_top + (k % 2) * cap, 16), cap)
+            x_back[k].start()
+        add_pair(j, own_top, wide)
 
     def finish(j):
-        x_back[j].wait_recv()
-        total[j] = (
-            pair[j, pl.ds(own_top, wide)].astype(jnp.float32) + chip_in[j].astype(jnp.float32)
-        ).astype(jnp.bfloat16)
-        home[2 * j].start()
-        home[2 * j + 1].start()
+        for k in (2 * j, 2 * j + 1):
+            x_back[k].wait_recv()
+            here = pl.ds((k % 2) * cap, cap)
+            held = pl.ds(pl.multiple_of(own_top + (k % 2) * cap, 16), cap)
+            total[j, here] = (
+                pair[j, held].astype(jnp.float32) + chip_in[j, here].astype(jnp.float32)
+            ).astype(jnp.bfloat16)
+            home[k].start()
 
     arrive(0)
     spread(0)
@@ -198,10 +210,10 @@
         home[k].wait()
     for k in range(experts):
         x_out[k].wait_send()
+        x_back[k].wait_send()
     for j in range(stages):
         d_out[j].wait_send()
         d_back[j].wait_send()
-        x_back[j].wait_send()
 
 
 def expert_half(
@@ -236,7 +248,7 @@
     bf16 = jnp.bfloat16
     dma = pltpu.SemaphoreType.DMA
     returned = pl.pallas_call(
-        functools.partial(expert_kernel, experts, shards, capacity, 256),
+        functools.partial(expert_kernel, experts, shards, capacity, 512),
         out_shape=jax.ShapeDtypeStruct((experts, capacity, features), bf16),
         in_specs=[pl.BlockSpec(memory_space=pltpu.VMEM)] + [pl.BlockSpec(memory_space=pl.ANY)] * 3,
         out_specs=pl.BlockSpec(memory_space=pltpu.VMEM),
@@ -255,8 +267,8 @@
             dma((2,)),
         ]
         + [dma((experts,))] * 4
-        + [dma((stages,))] * 6
-        + [dma((experts,))] * 2,
+        + [dma((stages,))] * 4
+        + [dma((experts,))] * 4,
         compiler_params=pltpu.CompilerParams(
             collective_id=0, has_side_effects=True, vmem_limit_bytes=60 * 2**20
         ),

time: 151 us -> 149 us (0.987)
  Pallas kernels: 116 us -> 113 us
    pallas_call x1, Pallas kernels: 116 us -> 113 us  [expert_half(): pl.pallas_call(functools.partial(expert_kernel, experts, shards, capacity...]
where the time goes in v2:
time: 149 us; the launch traced here: 148 us
  Pallas kernels  113 us (76%)
  between operations  14.2 us (10%)
  matrix products  7.31 us (5%)
  starting transfers between devices  6.86 us (5%)
  other arithmetic  5.52 us (4%)
    pallas_call x1, Pallas kernels, expert_half(): pl.pallas_call(functools.partial(expert_kernel, experts, shards, capacity...  113 us
    ppermute x1, starting transfers between devices, extended(): before = lax.ppermute(last, axis, up)  5.53 us
  transfers between devices with their start and end apart: 3, of which 0 were waited for; matrix products, arithmetic and copies ran while one was open for 6% of the time, Pallas kernels for 77%

profile of v2, /device:TPU:0, one launch (start us, length us, event | category | flops | bytes accessed | tf_op | source)
XLA Modules:
  0.0 148.0 jit_solution(10657339117806072523)
XLA Ops:
  7.2 0.0 copy-start
  7.2 0.0 copy-start.2
  7.2 0.0 reduce-scatter.2.cloned.1.call-start
  7.2 1.2 multiply_convert_fusion
  8.5 0.0 copy-start.4
  8.5 1.3 collective-permute-start.1
  9.8 5.5 %collective-permute-start = (bf16[1,256]{1,0:T(2,128)(2,1)S(1)}, bf16[1,256]{1,0:T(2,128)(2,1)S(1)}, u32[]{:S(2)}, u32[]{:S(2)}) collective-permute-start(bf16[1,256]{1,0:T(2,128)(2,1)S(1)} %get-tuple-element.6), channel_id=1, source_target_pairs={{0,4},{4,8},{8,12},{12,16},{16,20},{20,24},{24,28},{1,5},{5,9},{9,... | collective-permute-start | bytes 1544 | tf_op jit(solution)/shard_map/ppermute | solution.py:18
  15.3 0.7 fusion.20
  16.0 0.1 fusion.16
  16.1 0.7 select_reduce_fusion.1
  16.9 0.7 convert_add_fusion
  17.5 0.1 fusion.11
  17.6 0.7 convert_element_type.58
  18.3 1.2 fusion.1
  19.6 0.0 copy-start.3
  19.6 0.0 copy-done.2
  19.6 1.8 %convolution_convert_fusion.1 = bf16[384,2048]{1,0:T(8,128)(2,1)} fusion(pred[128,384]{1,0:T(8,128)(4,1)S(1)} %fusion.11, bf16[128,2048]{1,0:T(8,128)(2,1)S(1)} %copy-done.2, f32[2048]{0:T(1024)S(1)} %convert_element_type.58, f32[128]{0:T(128)S(1)} %add_rsqrt_fusion), kind=kOutput, calls=%fused_computation.1 | convolution fusion | flops 203161600 | bytes 2155008 | tf_op jit(solution)/shard_map/rs,rd->sd/dot_general | solution.py:243
  21.4 0.0 copy-done.4
  21.4 0.0 collective-permute-done.1
  21.4 0.0 collective-permute-done
  21.4 0.1 maximum_convert_fusion
  21.5 0.0 copy-done
  21.5 0.0 copy-done.3
  21.5 2.2 %convolution_convert_fusion = bf16[512,2048]{1,0:T(8,128)(2,1)} fusion(bf16[256,2048]{1,0:T(8,128)(2,1)S(1)} %copy-done, f32[514,256]{1,0:T(8,128)S(1)} %maximum_convert_fusion, bf16[512,256]{1,0:T(8,128)(2,1)S(1)} %copy-done.3, f32[256]{0:T(256)S(1)} %bitcast.18, f32[256]{0:T(256)S(1)} %bitcast.17, f32[256]{0:T(256)S(1)} %bitcast.16), kind=kOutput, calls=%fused_computation | convolution fusion | flops 538968064 | bytes 4983808 | tf_op jit(solution)/shard_map/dot_general | solution.py:34
  23.7 0.0 copy-start.5
  23.7 0.0 reduce-scatter.2.cloned.1.call-update
  23.7 0.7 copy-done.5
  24.4 0.1 select_reduce_fusion
  24.5 113.4 %shard_map.131 = bf16[8,48,2048]{2,1,0:T(8,128)(2,1)} custom-call(bf16[8,48,2048]{2,1,0:T(8,128)(2,1)} %bitcast.15, bf16[2048,1536]{1,0:T(8,128)(2,1)} %bitcast.19, bf16[2048,1536]{1,0:T(8,128)(2,1)} %bitcast.20, bf16[1536,2048]{1,0:T(8,128)(2,1)} %bitcast.21), custom_call_target="tpu_custom_call" | custom-call | flops 28991029248 | bytes 18874368 | tf_op jit(solution)/shard_map/pallas_call | solution.py:250
  137.9 0.0 copy-start.1
  137.9 2.0 %fusion.18 = f32[128,2048]{1,0:T(8,128)S(1)} fusion(bf16[384,2048]{1,0:T(8,128)(2,1)} %bitcast.13, f32[128,384]{1,0:T(8,128)S(1)} %select_reduce_fusion), kind=kOutput, calls=%fused_computation.30 | convolution fusion | flops 201375744 | bytes 2818048 | tf_op jit(solution)/shard_map/dot_general | solution.py:285
  139.9 0.0 copy-done.1
  139.9 1.2 fusion
  141.1 0.0 reduce-scatter.2.cloned.1.call-done
  (3 shorter events, 0.0 us)
Async XLA Ops:
  7.2 14.3 %copy-start = (bf16[256,2048]{1,0:T(8,128)(2,1)S(1)}, bf16[256,2048]{1,0:T(8,128)(2,1)}, u32[]{:S(2)}) copy-start(bf16[256,2048]{1,0:T(8,128)(2,1)} %param.16) | copy-start | bytes 3145732
  7.2 12.4 %copy-start.2 = (bf16[128,2048]{1,0:T(8,128)(2,1)S(1)}, bf16[128,2048]{1,0:T(8,128)(2,1)}, u32[]{:S(2)}) copy-start(bf16[128,2048]{1,0:T(8,128)(2,1)} %param.17) | copy-start | bytes 1572868
  7.2 134.0 %reduce-scatter.2.cloned.1.call-start = ((), (), s32[]{:S(2)}) async-start(), calls=%async_computation.1 | async-start | bytes 2621440 | tf_op jit(solution)/shard_map/reduce_scatter | solution.py:246
  8.5 13.0 %copy-start.4 = (bf16[3,256]{1,0:T(4,128)(2,1)S(1)}, bf16[3,256]{1,0:T(4,128)(2,1)}, u32[]{:S(2)}) copy-start(bf16[3,256]{1,0:T(4,128)(2,1)} %param.15) | copy-start | bytes 4612
  8.5 12.9 %collective-permute-start.1 = (bf16[1,256]{1,0:T(2,128)(2,1)S(1)}, bf16[1,256]{1,0:T(2,128)(2,1)S(1)}, u32[]{:S(2)}, u32[]{:S(2)}) collective-permute-start(bf16[1,256]{1,0:T(2,128)(2,1)S(1)} %get-tuple-element.7), channel_id=1, source_target_pairs={{4,0},{8,4},{12,8},{16,12},{20,16},{24,20},{28,24},{5,1},{9,5},{13... | collective-permute-start | bytes 1544 | tf_op jit(solution)/shard_map/ppermute | solution.py:19
  9.8 11.6 %collective-permute-start = (bf16[1,256]{1,0:T(2,128)(2,1)S(1)}, bf16[1,256]{1,0:T(2,128)(2,1)S(1)}, u32[]{:S(2)}, u32[]{:S(2)}) collective-permute-start(bf16[1,256]{1,0:T(2,128)(2,1)S(1)} %get-tuple-element.6), channel_id=1, source_target_pairs={{0,4},{4,8},{8,12},{12,16},{16,20},{20,24},{24,28},{1,5},{5,9},{9,... | collective-permute-start | bytes 1544 | tf_op jit(solution)/shard_map/ppermute | solution.py:18
  19.6 1.9 %copy-start.3 = (bf16[512,256]{1,0:T(8,128)(2,1)S(1)}, bf16[512,256]{1,0:T(8,128)(2,1)}, u32[]{:S(2)}) copy-start(bf16[512,256]{1,0:T(8,128)(2,1)} %param.14) | copy-start | bytes 786436
  23.7 0.7 copy-start.5
  137.9 2.0 %copy-start.1 = (bf16[8,48,2048]{2,1,0:T(8,128)(2,1)S(1)}, bf16[8,48,2048]{2,1,0:T(8,128)(2,1)}, u32[]{:S(2)}) copy-start(bf16[8,48,2048]{2,1,0:T(8,128)(2,1)} %shard_map.131) | copy-start | bytes 4718596
Sparse Core Ops, SparseCore 0:
  23.8 38.1 reduce-scatter.1
